TPU v7x, 128 devices: a whole 4x4x4 slice. The times are simulated.
128 devices in a mesh: sp: 16 (over z, x), tp: 8 (over y, core).
Axes of the slice: x: 4, y: 4, z: 4, core: 2. Of those that a mesh axis runs over, the one named last changes fastest.
Arguments:
- resid: bfloat16 [12288, 2048], P(('sp', 'tp')), may hold values from -6 to 6
- queries: bfloat16 [12288, 1024], P('sp', 'tp'), may hold values from -160 to 160
- keys: bfloat16 [12288, 1024], P('sp', 'tp'), may hold values from -6 to 6
- values: bfloat16 [12288, 1024], P('sp', 'tp'), may hold values from -6 to 6
- cum_gate: float32 [12288, 16], P('sp', 'tp'), may hold values from -1385 to 0, as said below
- out_weight: bfloat16 [1024, 2048], P('tp'), may hold values from -0.375 to 0.375
- norm_gain: float32 [2048], replicated, may hold values from 0.1 to 1.9
- gate_weight: bfloat16 [2048, 5504], P('sp', 'tp'), may hold values from -0.125 to 0.125
- up_weight: bfloat16 [2048, 5504], P('sp', 'tp'), may hold values from -0.125 to 0.125
- down_weight: bfloat16 [5504, 2048], P('tp', 'sp'), may hold values from -0.078125 to 0.078125
Outputs:
- layer_out: bfloat16 [12288, 2048], P(('sp', 'tp'))
Inputs may be any that keep to these rules, and one draw needn't show every extreme that they name: `cum_gate`: each column is non-increasing along positions and starts at or below zero.
All inputs are finite; a program needn't handle non-finite values.
Results may differ from a plain program's by a relative error of at most 0.01.
Values may be sent and summed in bfloat16 or wider, within the bound.
A program may use at most 256 MiB of HBM per device.

v0:
```python
import jax
import jax.numpy as jnp
from jax import lax
from jax.sharding import Mesh
from jax.sharding import PartitionSpec as P

HEAD_DIM = 64
TP = ("tp_0", "tp_1")
SP_TP = ("sp", "tp_0", "tp_1")


def turned_gather(arrays, axis, dims):
    turned = [jnp.moveaxis(a, dim, 0) for a, dim in zip(arrays, dims)]
    widths = [t[0].size for t in turned]
    both = jnp.concatenate([t.reshape(-1, w) for t, w in zip(turned, widths)], axis=1)
    out = lax.all_gather(both, axis, axis=0, tiled=True)
    blocks = jnp.split(out, [sum(widths[:k]) for k in range(1, len(widths))], axis=1)
    return tuple(
        (
            jnp.moveaxis(b.reshape(-1, *t.shape[1:]), 0, dim)
            for b, t, dim in zip(blocks, turned, dims)
        )
    )


def joined_along(blocks, dim):
    blocks = jnp.moveaxis(blocks, 0, dim)
    lengths = blocks.shape
    return blocks.reshape(*lengths[:dim], lengths[dim] * lengths[dim + 1], *lengths[dim + 2 :])


def copy_for_each(value, axis):
    count = lax.axis_size(axis)
    return lax.all_to_all(
        jnp.broadcast_to(value[None], (count, *value.shape)), axis, 0, 0, tiled=True
    )


def gathered_copies(value, axis, dim):
    return joined_along(copy_for_each(value, axis), dim)


def sent_together(arrays, axis, dim, along):
    ends, at = ([], 0)
    for a in arrays[:-1]:
        at += a.shape[along]
        ends.append(at)
    both = jnp.concatenate(arrays, axis=along)
    return tuple(jnp.split(lax.all_gather(both, axis, axis=dim, tiled=True), ends, axis=along))


def sum_by_axis(value, axes, dim):
    for axis in axes:
        value = lax.psum_scatter(value, axis, scatter_dimension=dim, tiled=True)
    return value


def rms_norm(mixed, norm_gain):
    scaled = mixed * lax.rsqrt(jnp.mean(mixed * mixed, axis=-1, keepdims=True) + 1e-06) * norm_gain
    return scaled.astype(jnp.bfloat16)


def rounded(term):
    return term.astype(jnp.bfloat16).astype(jnp.float32)


def local(
    resid,
    queries,
    keys,
    values,
    cum_gate,
    out_weight,
    norm_gain,
    gate_weight,
    up_weight,
    down_weight,
):
    rows = queries.shape[0]
    heads_here = cum_gate.shape[1]
    scale = HEAD_DIM ** (-0.5)
    whole_gate, whole_up, whole_down = turned_gather(
        (gate_weight, up_weight, down_weight), "sp", (0, 0, 1)
    )
    proj_weight = lax.all_gather(out_weight, TP, axis=0, tiled=True)
    first = lax.axis_index("sp") * rows
    gates_all = gathered_copies(cum_gate, "sp", 0)
    query_heads = queries.reshape(rows, heads_here, HEAD_DIM)
    query_pos = first + jnp.arange(rows, dtype=jnp.int32)
    query_gate = cum_gate.T
    best = jnp.full((heads_here, rows), -1e30, jnp.float32)
    key_piece, value_piece = sent_together((keys, values), "sp", 0, 1)
    count = key_piece.shape[0]
    key_heads = key_piece.reshape(count, heads_here, HEAD_DIM)
    value_heads = value_piece.reshape(count, heads_here, HEAD_DIM)
    key_gate = gates_all.T
    score = (
        jnp.einsum("qhd,khd->hqk", query_heads, key_heads, preferred_element_type=jnp.float32)
        * scale
    )
    score = score + query_gate[:, :, None] - key_gate[:, None, :]
    key_pos = jnp.arange(count, dtype=jnp.int32)
    score = jnp.where(key_pos[None, None, :] <= query_pos[None, :, None], score, -jnp.inf)
    new_best = jnp.maximum(best, jnp.max(score, axis=-1))
    weight = jnp.exp(score - new_best[:, :, None])
    total = jnp.sum(weight, axis=-1)
    numer = jnp.einsum(
        "hqk,khd->hqd", weight.astype(jnp.bfloat16), value_heads, preferred_element_type=jnp.float32
    )
    best, total, numer = (new_best, total, numer)
    attn = (
        (numer / total[:, :, None])
        .transpose(1, 0, 2)
        .reshape(rows, heads_here * HEAD_DIM)
        .astype(jnp.bfloat16)
    )
    groups = lax.axis_size(TP)
    share = rows // groups
    own_rows = lax.all_to_all(attn, TP, split_axis=0, concat_axis=1, tiled=True)
    group_width = attn.shape[1]
    row_groups = own_rows.reshape(share, groups, group_width)
    weight_groups = proj_weight.reshape(groups, group_width, proj_weight.shape[1])
    terms = jnp.einsum(
        "rgc,gcd->grd", row_groups, weight_groups, preferred_element_type=jnp.float32
    )
    proj = jnp.sum(rounded(terms), axis=0)
    mixed = resid.astype(jnp.float32) + proj
    normed_all = lax.all_gather(rms_norm(mixed, norm_gain), TP, axis=0, tiled=True)
    gate = jnp.dot(normed_all, whole_gate, preferred_element_type=jnp.float32)
    upper = jnp.dot(normed_all, whole_up, preferred_element_type=jnp.float32)
    hidden = (jax.nn.silu(gate) * upper).astype(jnp.bfloat16)
    ffn_part = jnp.dot(hidden, whole_down, preferred_element_type=jnp.float32)
    ffn = sum_by_axis(rounded(ffn_part).astype(jnp.bfloat16), TP, 0).astype(jnp.float32)
    return (mixed + 0.5 * ffn).astype(jnp.bfloat16)


def solution(mesh):
    split = Mesh(mesh.devices.reshape(mesh.shape["sp"], 4, 2), ("sp", "tp_0", "tp_1"))
    return jax.shard_map(
        local,
        mesh=split,
        in_specs=(
            P(SP_TP, None),
            P("sp", TP),
            P("sp", TP),
            P("sp", TP),
            P("sp", TP),
            P(TP, None),
            P(),
            P("sp", TP),
            P("sp", TP),
            P(TP, "sp"),
        ),
        out_specs=P(SP_TP, None),
        check_vma=False,
    )
```

profile of v0, /device:TPU:1, one launch (start us, length us, event | category | flops | bytes accessed | tf_op | source)
XLA Modules:
  0.0 297.3 jit_solution(10596566933157385455)
XLA Ops:
  6.5 0.0 all-gather.5.cloned.1.call-start
  6.5 1.8 pad_maximum_fusion.1
  8.3 0.0 copy-start.2
  8.3 0.0 all-gather.5.cloned.1.call-update
  8.4 0.0 all-gather.7.cloned.1.call-start
  8.4 0.7 all-gather.7.cloned.1.call-update
  9.1 1.4 broadcast_in_dim.17
  10.5 8.4 %all-to-all-start = ((f32[16,768,2]{1,2,0:T(2,128)}), f32[16,768,2]{1,2,0:T(2,128)S(1)}, u32[]{:S(2)}, u32[]{:S(2)}) async-start(f32[16,768,2]{1,2,0:T(2,128)} %broadcast_in_dim.17), calls=%async_computation | async-start | bytes 196608 | tf_op jit(solution)/shard_map/all_to_all | solution.py:34
  18.9 0.0 all-gather.11.cloned.1.call-start
  19.0 1.9 pad_maximum_fusion
  20.9 0.0 all-gather.11.cloned.1.call-update
  20.9 7.4 %iota_compare_fusion = pred[768,12288]{0,1:T(8,128)(4,1)} fusion(s32[768]{0:T(1024)S(1)} %iota_add_fusion), kind=kLoop, calls=%fused_computation.5 | loop fusion | flops 9437184 | bytes 9440256 | tf_op jit(solution)/shard_map/le | solution.py:103
  28.3 0.0 copy-done.2
  28.3 0.1 copy.22
  28.4 45.5 %all-gather.5.cloned.1.call-done = bf16[12288,256]{1,0:T(8,128)(2,1)} async-done(((bf16[768,256]{1,0:T(8,128)(2,1)}), bf16[12288,256]{1,0:T(8,128)(2,1)}) %all-gather.5.cloned.1.call-update) | async-done | bytes 6291472 | tf_op jit(solution)/shard_map/all_gather | solution.py:49
  73.9 4.3 %fusion.29 = (bf16[12288,128]{1,0:T(8,128)(2,1)}, bf16[12288,128]{1,0:T(8,128)(2,1)S(1)}) fusion(bf16[12288,256]{1,0:T(8,128)(2,1)} %all-gather.5.cloned.1.call-done), kind=kLoop, calls=%fused_computation.34 | loop fusion | bytes 12582912 | tf_op jit(solution)/shard_map/split | solution.py:49
  78.2 0.0 copy-start.3
  78.2 4.7 %copy.21 = bf16[12288,128]{0,1:T(8,128)(2,1)} copy(bf16[12288,128]{1,0:T(8,128)(2,1)} %get-tuple-element.5) | data formatting | bytes 6291456 | tf_op jit(solution)/shard_map/split | solution.py:49
  82.9 0.0 all-to-all-done
  83.0 0.0 copy-done.3
  83.0 33.3 %fusion.2 = (f32[2,768]{1,0:T(2,128)S(1)}, f32[2,12288,768]{2,1,0:T(8,128)}) fusion(f32[2,12288]{1,0:T(2,128)S(1)} %bitcast.45, f32[2,768]{1,0:T(2,128)S(1)} %bitcast.50, pred[768,12288]{0,1:T(8,128)(4,1)} %iota_compare_fusion, bf16[12288,2,64]{0,2,1:T(8,128)(2,1)} %bitcast.43, bf16[768,2,64]{0,2,1:T(8,128)(2,1)S(1)} %bitcast.48), kind=kOutput, calls=%fused_computation.4 | convolution fusion | flops 2510289408 | bytes 88387584 | tf_op jit(solution)/shard_map/qhd,khd->hqk/dot_general | solution.py:98
  116.2 2.8 copy.23
  119.1 0.0 copy-start.1
  119.1 27.7 %fusion = f32[2,768]{1,0:T(2,128)S(1)} fusion(f32[2,12288,768]{2,1,0:T(8,128)} %get-tuple-element.8, f32[2,768]{1,0:T(2,128)S(1)} %broadcast_maximum_fusion, f32[2,12288]{1,0:T(2,128)S(1)} %bitcast.46, f32[2,768]{1,0:T(2,128)S(1)} %bitcast.51, pred[768,12288]{0,1:T(8,128)(4,1)} %iota_compare_fusion), kind=kLoop, calls=%fused_computation.2 | loop fusion | flops 113244672 | bytes 85051392 | tf_op jit(solution)/shard_map/reduce_sum | solution.py:106
  146.8 0.0 copy-done.1
  146.8 30.7 %fusion.22 = bf16[768,2,64]{0,2,1:T(8,128)(2,1)S(1)} fusion(bf16[12288,2,64]{0,2,1:T(8,128)(2,1)S(1)} %bitcast.44, f32[2,12288,768]{2,1,0:T(8,128)} %get-tuple-element.8, f32[2,768]{1,0:T(2,128)S(1)} %broadcast_maximum_fusion, f32[2,12288]{1,0:T(2,128)S(1)} %bitcast.47, f32[2,768]{1,0:T(2,128)S(1)} %bitcast.52, pred[768,12288]{0,1:T(8,128)(4,1)} %iota_compare_fusion, ...), kind=kOutput, calls=%fused_computation.20 | convolution fusion | flops 2529361920 | bytes 88393728 | tf_op jit(solution)/shard_map/hqk,khd->hqd/dot_general | solution.py:107
  177.5 0.0 copy-start
  177.5 0.0 copy-start.4
  177.5 0.3 convert_element_type.39
  177.8 0.9 copy.25
  178.7 5.0 %all-to-all-start.1 = ((bf16[8,96,128]{2,1,0:T(8,128)(2,1)}), bf16[8,96,128]{2,1,0:T(8,128)(2,1)S(1)}, u32[]{:S(2)}, u32[]{:S(2)}) async-start(bf16[8,96,128]{2,1,0:T(8,128)(2,1)} %copy.25), calls=%async_computation.1 | async-start | bytes 393216 | tf_op jit(solution)/shard_map/all_to_all | solution.py:119
  183.7 0.0 all-gather.9.cloned.1.call-start
  183.8 0.0 all-gather.7.cloned.1.call-done
  183.8 5.9 %all-to-all-done.1 = bf16[8,96,128]{2,1,0:T(8,128)(2,1)S(1)} async-done(((bf16[8,96,128]{2,1,0:T(8,128)(2,1)}), bf16[8,96,128]{2,1,0:T(8,128)(2,1)S(1)}, u32[]{:S(2)}, u32[]{:S(2)}) %all-to-all-start.1) | async-done | bytes 196640 | tf_op jit(solution)/shard_map/all_to_all | solution.py:119
  189.6 3.2 %convert_reduce_fusion = f32[96,2048]{1,0:T(8,128)S(1)} fusion(bf16[8,128,2048]{2,1,0:T(8,128)(2,1)} %bitcast.42, bf16[8,96,128]{2,1,0:T(8,128)(2,1)S(1)} %all-to-all-done.1), kind=kOutput, calls=%fused_computation.8 | convolution fusion | flops 407175168 | bytes 5177344 | tf_op jit(solution)/shard_map/rgc,gcd->grd/dot_general | solution.py:123
  192.8 0.0 copy-done
  192.8 0.2 multiply_reduce_fusion
  193.0 0.0 copy-done.4
  193.0 0.9 multiply_convert_fusion.1
  193.9 0.0 all-gather.9.cloned.1.call-update
  193.9 0.2 reduce-scatter.3.cloned.1.call-start
  194.2 0.0 all-gather.11.cloned.1.call-done
  194.2 26.3 %all-gather.9.cloned.1.call-done = bf16[768,2048]{1,0:T(8,128)(2,1)} async-done(((bf16[96,2048]{1,0:T(8,128)(2,1)}), bf16[768,2048]{1,0:T(8,128)(2,1)}) %all-gather.9.cloned.1.call-update) | async-done | bytes 3145744 | tf_op jit(solution)/shard_map/all_gather | solution.py:128
  220.5 5.1 %fusion.9 = f32[768,688]{0,1:T(8,128)S(1)} fusion(bf16[768,2048]{1,0:T(8,128)(2,1)} %all-gather.9.cloned.1.call-done, bf16[2048,2064]{0,1:T(8,128)(2,1)} %all-gather.11.cloned.1.call-done), kind=kOutput, calls=%fused_computation.14 | convolution fusion | flops 2164260864 | bytes 8077312 | tf_op jit(solution)/shard_map/dot_general | solution.py:129
  225.6 11.7 %convolution_convert_fusion = bf16[768,2048]{1,0:T(8,128)(2,1)} fusion(bf16[2048,2064]{0,1:T(8,128)(2,1)} %all-gather.11.cloned.1.call-done, f32[768,688]{0,1:T(8,128)S(1)} %fusion.9, bf16[768,2048]{1,0:T(8,128)(2,1)} %all-gather.9.cloned.1.call-done), kind=kOutput, calls=%fused_computation.9 | convolution fusion | flops 4333264896 | bytes 14041088 | tf_op jit(solution)/shard_map/dot_general | solution.py:132
  237.3 0.0 reduce-scatter.3.cloned.1.call-update
  237.3 0.0 reduce-scatter.5.cloned.1.call-start
  237.4 37.9 %reduce-scatter.3.cloned.1.call-done = bf16[192,2048]{1,0:T(8,128)(2,1)} async-done(((bf16[768,2048]{1,0:T(8,128)(2,1)}), bf16[192,2048]{1,0:T(8,128)(2,1)}) %reduce-scatter.3.cloned.1.call-update) | async-done | bytes 786448 | tf_op jit(solution)/shard_map/reduce_scatter | solution.py:54
  275.2 0.0 reduce-scatter.5.cloned.1.call-update
  275.3 13.3 %reduce-scatter.5.cloned.1.call-done = bf16[96,2048]{1,0:T(8,128)(2,1)} async-done(((bf16[192,2048]{1,0:T(8,128)(2,1)}), bf16[96,2048]{1,0:T(8,128)(2,1)}) %reduce-scatter.5.cloned.1.call-update) | async-done | bytes 393232 | tf_op jit(solution)/shard_map/reduce_scatter | solution.py:54
  288.6 1.9 add_convert_fusion
  (3 shorter events, 0.0 us)
Async XLA Ops:
  6.5 67.4 %all-gather.5.cloned.1.call-start = ((), (), s32[]{:S(2)}) async-start(), calls=%async_computation.4 | async-start | bytes 6684672 | tf_op jit(solution)/shard_map/all_gather | solution.py:49
  8.3 19.9 %copy-start.2 = (bf16[768,128]{1,0:T(8,128)(2,1)S(1)}, bf16[768,128]{1,0:T(8,128)(2,1)}, u32[]{:S(2)}) copy-start(bf16[768,128]{1,0:T(8,128)(2,1)} %param.11) | copy-start | bytes 589828
  8.4 175.4 %all-gather.7.cloned.1.call-start = ((), (), s32[]{:S(2)}) async-start(), calls=%async_computation.5 | async-start | bytes 4718592 | tf_op jit(solution)/shard_map/all_gather | solution.py:85
  10.5 72.5 %all-to-all-start = ((f32[16,768,2]{1,2,0:T(2,128)}), f32[16,768,2]{1,2,0:T(2,128)S(1)}, u32[]{:S(2)}, u32[]{:S(2)}) async-start(f32[16,768,2]{1,2,0:T(2,128)} %broadcast_in_dim.17), calls=%async_computation | async-start | bytes 196608 | tf_op jit(solution)/shard_map/all_to_all | solution.py:34
  18.9 175.3 %all-gather.11.cloned.1.call-start = ((), (), s32[]{:S(2)}) async-start(), calls=%async_computation.7 | async-start | bytes 8982528 | tf_op jit(solution)/shard_map/all_gather | solution.py:16
  78.2 4.7 %copy-start.3 = (f32[768,2]{0,1:T(2,128)S(1)}, f32[768,2]{0,1:T(2,128)}, u32[]{:S(2)}) copy-start(f32[768,2]{0,1:T(2,128)} %param.14) | copy-start | bytes 18436
  119.1 27.8 %copy-start.1 = (bf16[12288,128]{0,1:T(8,128)(2,1)S(1)}, bf16[12288,128]{0,1:T(8,128)(2,1)}, u32[]{:S(2)}) copy-start(bf16[12288,128]{0,1:T(8,128)(2,1)} %copy.23) | copy-start | bytes 9437188
  177.5 15.3 %copy-start = (bf16[96,2048]{1,0:T(8,128)(2,1)S(1)}, bf16[96,2048]{1,0:T(8,128)(2,1)}, u32[]{:S(2)}) copy-start(bf16[96,2048]{1,0:T(8,128)(2,1)} %param.10) | copy-start | bytes 1179652
  177.5 15.5 %copy-start.4 = (f32[2048]{0:T(1024)S(1)}, f32[2048]{0:T(1024)}, u32[]{:S(2)}) copy-start(f32[2048]{0:T(1024)} %param.16) | copy-start | bytes 24580
  178.7 10.9 %all-to-all-start.1 = ((bf16[8,96,128]{2,1,0:T(8,128)(2,1)}), bf16[8,96,128]{2,1,0:T(8,128)(2,1)S(1)}, u32[]{:S(2)}, u32[]{:S(2)}) async-start(bf16[8,96,128]{2,1,0:T(8,128)(2,1)} %copy.25), calls=%async_computation.1 | async-start | bytes 393216 | tf_op jit(solution)/shard_map/all_to_all | solution.py:119
  183.7 36.7 %all-gather.9.cloned.1.call-start = ((), (), s32[]{:S(2)}) async-start(), calls=%async_computation.6 | async-start | bytes 3538944 | tf_op jit(solution)/shard_map/all_gather | solution.py:128
  193.9 81.3 %reduce-scatter.3.cloned.1.call-start = ((), (), s32[]{:S(2)}) async-start(), calls=%async_computation.8 | async-start | bytes 3932160 | tf_op jit(solution)/shard_map/reduce_scatter | solution.py:54
  237.3 51.2 %reduce-scatter.5.cloned.1.call-start = ((), (), s32[]{:S(2)}) async-start(), calls=%async_computation.9 | async-start | bytes 1179648 | tf_op jit(solution)/shard_map/reduce_scatter | solution.py:54
Sparse Core Ops, SparseCore 0:
  9.5 64.4 all-gather.4
  75.7 32.1 all-gather.6
  110.0 75.8 all-gather.10
  194.1 26.3 all-gather.8
  237.5 37.7 reduce-scatter.2
  277.4 11.0 reduce-scatter.4
where the time goes:
time: 298 us; the launch traced here: 297 us
  waiting for transfers between devices  130 us (44%)
  matrix products  83.9 us (28%)
  other arithmetic  41.8 us (14%)
  local copies, waits for them, and re-layouts  14.5 us (5%)
  starting transfers between devices  13.8 us (5%)
  between operations  13.6 us (5%)
    reduce_scatter x2, waiting for transfers between devices, sum_by_axis(): value = lax.psum_scatter(value, axis, scatter_dimension=dim, tiled=True)  51.1 us
    all_gather x1, waiting for transfers between devices, sent_together(): lax.all_gather(both, axis, axis=dim, tiled=True)  45.5 us
    dot_general x1, matrix products, local(): jnp.einsum('qhd,khd->hqk', query_heads, key_heads, preferred_element_type...  33.3 us
    dot_general x1, matrix products, local(): jnp.einsum('hqk,khd->hqd', weight.astype(jnp.bfloat16), value_heads, pref...  30.7 us
    reduce_sum x1, other arithmetic, local(): total = jnp.sum(weight, axis=-1)  27.7 us
    all_gather x1, waiting for transfers between devices, local(): lax.all_gather(rms_norm(mixed, norm_gain), TP, axis=0, tiled=True)  26.3 us
    split x3, local copies, waits for them, and re-layouts, sent_together(): jnp.split(lax.all_gather(both, axis, axis=dim, tiled=True), ends, axis=al...  11.8 us
    dot_general x1, matrix products, local(): ffn_part = jnp.dot(hidden, whole_down, preferred_element_type=jnp.float32)  11.7 us
  transfers between devices with their start and end apart: 8, of which 5 were waited for; matrix products, arithmetic and copies ran while one was open for 40% of the time, Pallas kernels for 0%

commit v1 on v0

--- a/solution.py
+++ b/solution.py
@@ -3,6 +3,7 @@
 from jax import lax
 from jax.sharding import Mesh
 from jax.sharding import PartitionSpec as P
+from jax.lax import all_to_all, psum
 
 HEAD_DIM = 64
 TP = ("tp_0", "tp_1")
@@ -125,7 +126,9 @@
     )
     proj = jnp.sum(rounded(terms), axis=0)
     mixed = resid.astype(jnp.float32) + proj
-    normed_all = lax.all_gather(rms_norm(mixed, norm_gain), TP, axis=0, tiled=True)
+    normed_all = jnp.concatenate(
+        all_to_all(jnp.stack([rms_norm(mixed, norm_gain)] * psum(1, TP), axis=0), TP, 0, 0), axis=0
+    )
     gate = jnp.dot(normed_all, whole_gate, preferred_element_type=jnp.float32)
     upper = jnp.dot(normed_all, whole_up, preferred_element_type=jnp.float32)
     hidden = (jax.nn.silu(gate) * upper).astype(jnp.bfloat16)

time: 298 us -> 311 us (1.044)
  blocking collectives: 0 us -> 41.6 us
  waiting for transfers between devices: 130 us -> 102 us
    all_to_all x0 -> x1, blocking collectives: none -> 41.6 us  [local(): all_to_all(jnp.stack([rms_norm(mixed, norm_gain)] * psum(1, TP), axis=0),...]
    all_gather x1 -> x0, waiting for transfers between devices: 26.3 us -> none  [local(): lax.all_gather(rms_norm(mixed, norm_gain), TP, axis=0, tiled=True)]
  transfers between devices with their start and end apart: 8 -> 7, of which waited for: 5 -> 4; matrix products, arithmetic and copies ran while one was open for 40% -> 38% of each run, Pallas kernels for 0% -> 0%
where the time goes in v1:
time: 311 us; the launch traced here: 310 us
  waiting for transfers between devices  102 us (33%)
  matrix products  84 us (27%)
  blocking collectives  41.6 us (13%)
  other arithmetic  41.1 us (13%)
  local copies, waits for them, and re-layouts  14.9 us (5%)
  starting transfers between devices  13.6 us (4%)
  between operations  13.3 us (4%)
    reduce_scatter x2, waiting for transfers between devices, sum_by_axis(): value = lax.psum_scatter(value, axis, scatter_dimension=dim, tiled=True)  50 us
    all_gather x1, waiting for transfers between devices, sent_together(): lax.all_gather(both, axis, axis=dim, tiled=True)  45.5 us
    all_to_all x1, blocking collectives, local(): all_to_all(jnp.stack([rms_norm(mixed, norm_gain)] * psum(1, TP), axis=0),...  41.6 us
    dot_general x1, matrix products, local(): jnp.einsum('qhd,khd->hqk', query_heads, key_heads, preferred_element_type...  33.3 us
    dot_general x1, matrix products, local(): jnp.einsum('hqk,khd->hqd', weight.astype(jnp.bfloat16), value_heads, pref...  30.7 us
    reduce_sum x1, other arithmetic, local(): total = jnp.sum(weight, axis=-1)  27.8 us
    split x3, local copies, waits for them, and re-layouts, sent_together(): jnp.split(lax.all_gather(both, axis, axis=dim, tiled=True), ends, axis=al...  11.8 us
    dot_general x1, matrix products, local(): ffn_part = jnp.dot(hidden, whole_down, preferred_element_type=jnp.float32)  11.7 us
  transfers between devices with their start and end apart: 7, of which 4 were waited for; matrix products, arithmetic and copies ran while one was open for 38% of the time, Pallas kernels for 0%

profile of v1, /device:TPU:1, one launch (start us, length us, event | category | flops | bytes accessed | tf_op | source)
XLA Modules:
  0.0 310.4 jit_solution(7463301329667845432)
XLA Ops:
  6.5 0.0 all-gather.4.cloned.1.call-start
  6.5 1.8 pad_maximum_fusion.1
  8.3 0.0 copy-start.2
  8.3 0.0 all-gather.4.cloned.1.call-update
  8.4 0.0 all-gather.6.cloned.1.call-start
  8.4 0.7 all-gather.6.cloned.1.call-update
  9.1 1.4 broadcast_in_dim.17
  10.5 8.4 %all-to-all-start = ((f32[16,768,2]{1,2,0:T(2,128)}), f32[16,768,2]{1,2,0:T(2,128)S(1)}, u32[]{:S(2)}, u32[]{:S(2)}) async-start(f32[16,768,2]{1,2,0:T(2,128)} %broadcast_in_dim.17), calls=%async_computation | async-start | bytes 196608 | tf_op jit(solution)/shard_map/all_to_all | solution.py:35
  18.9 0.0 all-gather.8.cloned.1.call-start
  19.0 1.9 pad_maximum_fusion
  20.9 0.0 all-gather.8.cloned.1.call-update
  20.9 7.4 %iota_compare_fusion = pred[768,12288]{0,1:T(8,128)(4,1)} fusion(s32[768]{0:T(1024)S(1)} %iota_add_fusion), kind=kLoop, calls=%fused_computation.5 | loop fusion | flops 9437184 | bytes 9440256 | tf_op jit(solution)/shard_map/le | solution.py:104
  28.3 0.0 copy-done.2
  28.3 0.1 copy.22
  28.5 45.5 %all-gather.4.cloned.1.call-done = bf16[12288,256]{1,0:T(8,128)(2,1)} async-done(((bf16[768,256]{1,0:T(8,128)(2,1)}), bf16[12288,256]{1,0:T(8,128)(2,1)}) %all-gather.4.cloned.1.call-update) | async-done | bytes 6291472 | tf_op jit(solution)/shard_map/all_gather | solution.py:50
  73.9 4.3 %fusion.29 = (bf16[12288,128]{1,0:T(8,128)(2,1)}, bf16[12288,128]{1,0:T(8,128)(2,1)S(1)}) fusion(bf16[12288,256]{1,0:T(8,128)(2,1)} %all-gather.4.cloned.1.call-done), kind=kLoop, calls=%fused_computation.34 | loop fusion | bytes 12582912 | tf_op jit(solution)/shard_map/split | solution.py:50
  78.2 0.0 copy-start.3
  78.2 4.7 %copy.21 = bf16[12288,128]{0,1:T(8,128)(2,1)} copy(bf16[12288,128]{1,0:T(8,128)(2,1)} %get-tuple-element.5) | data formatting | bytes 6291456 | tf_op jit(solution)/shard_map/split | solution.py:50
  82.9 0.0 all-to-all-done
  82.9 0.0 copy-done.3
  82.9 33.3 %fusion.2 = (f32[2,768]{1,0:T(2,128)S(1)}, f32[2,12288,768]{2,1,0:T(8,128)}) fusion(f32[2,12288]{1,0:T(2,128)S(1)} %bitcast.48, f32[2,768]{1,0:T(2,128)S(1)} %bitcast.53, pred[768,12288]{0,1:T(8,128)(4,1)} %iota_compare_fusion, bf16[12288,2,64]{0,2,1:T(8,128)(2,1)} %bitcast.44, bf16[768,2,64]{0,2,1:T(8,128)(2,1)S(1)} %bitcast.51), kind=kOutput, calls=%fused_computation.4 | convolution fusion | flops 2510289408 | bytes 88387584 | tf_op jit(solution)/shard_map/qhd,khd->hqk/dot_general | solution.py:99
  116.2 2.8 copy.23
  119.0 0.0 copy-start.1
  119.0 27.8 %fusion = f32[2,768]{1,0:T(2,128)S(1)} fusion(f32[2,12288,768]{2,1,0:T(8,128)} %get-tuple-element.8, f32[2,768]{1,0:T(2,128)S(1)} %broadcast_maximum_fusion, f32[2,12288]{1,0:T(2,128)S(1)} %bitcast.49, f32[2,768]{1,0:T(2,128)S(1)} %bitcast.54, pred[768,12288]{0,1:T(8,128)(4,1)} %iota_compare_fusion), kind=kLoop, calls=%fused_computation.2 | loop fusion | flops 113244672 | bytes 85051392 | tf_op jit(solution)/shard_map/reduce_sum | solution.py:107
  146.8 0.0 copy-done.1
  146.8 30.7 %fusion.22 = bf16[768,2,64]{0,2,1:T(8,128)(2,1)S(1)} fusion(bf16[12288,2,64]{0,2,1:T(8,128)(2,1)S(1)} %bitcast.45, f32[2,12288,768]{2,1,0:T(8,128)} %get-tuple-element.8, f32[2,768]{1,0:T(2,128)S(1)} %broadcast_maximum_fusion, f32[2,12288]{1,0:T(2,128)S(1)} %bitcast.50, f32[2,768]{1,0:T(2,128)S(1)} %bitcast.55, pred[768,12288]{0,1:T(8,128)(4,1)} %iota_compare_fusion, ...), kind=kOutput, calls=%fused_computation.20 | convolution fusion | flops 2529361920 | bytes 88393728 | tf_op jit(solution)/shard_map/hqk,khd->hqd/dot_general | solution.py:108
  177.5 0.0 copy-start
  177.5 0.0 copy-start.4
  177.5 0.3 convert_element_type.39
  177.8 0.9 copy.25
  178.7 5.1 %all-to-all-start.1 = ((bf16[8,96,128]{2,1,0:T(8,128)(2,1)}), bf16[8,96,128]{2,1,0:T(8,128)(2,1)S(1)}, u32[]{:S(2)}, u32[]{:S(2)}) async-start(bf16[8,96,128]{2,1,0:T(8,128)(2,1)} %copy.25), calls=%async_computation.1 | async-start | bytes 393216 | tf_op jit(solution)/shard_map/all_to_all | solution.py:120
  183.7 0.0 reduce-scatter.3.cloned.1.call-start
  183.7 0.0 all-gather.6.cloned.1.call-done
  183.7 5.9 %all-to-all-done.1 = bf16[8,96,128]{2,1,0:T(8,128)(2,1)S(1)} async-done(((bf16[8,96,128]{2,1,0:T(8,128)(2,1)}), bf16[8,96,128]{2,1,0:T(8,128)(2,1)S(1)}, u32[]{:S(2)}, u32[]{:S(2)}) %all-to-all-start.1) | async-done | bytes 196640 | tf_op jit(solution)/shard_map/all_to_all | solution.py:120
  189.6 3.2 %convert_reduce_fusion = f32[96,2048]{1,0:T(8,128)S(1)} fusion(bf16[8,128,2048]{2,1,0:T(8,128)(2,1)} %bitcast.43, bf16[8,96,128]{2,1,0:T(8,128)(2,1)S(1)} %all-to-all-done.1), kind=kOutput, calls=%fused_computation.8 | convolution fusion | flops 407175168 | bytes 5177344 | tf_op jit(solution)/shard_map/rgc,gcd->grd/dot_general | solution.py:124
  192.8 0.0 copy-done
  192.8 0.2 multiply_reduce_fusion
  193.0 0.0 copy-done.4
  193.0 0.1 multiply_convert_fusion.1
  193.2 0.4 stack.2
  193.6 41.6 %all_to_all.23 = bf16[8,96,2048]{2,1,0:T(8,128)(2,1)} all-to-all(bf16[8,96,2048]{2,1,0:T(8,128)(2,1)S(1)} %stack.2), channel_id=1, replica_groups=mesh['sp'=16,'tp_0'=4,'tp_1'=2] {'tp_0','tp_1'}, dimensions={0} | all-to-all | bytes 6291456 | tf_op jit(solution)/shard_map/all_to_all | solution.py:130
  235.1 0.0 all-gather.8.cloned.1.call-done
  235.1 5.1 %fusion.9 = f32[768,688]{0,1:T(8,128)S(1)} fusion(bf16[768,2048]{1,0:T(8,128)(2,1)} %bitcast.46, bf16[2048,2064]{0,1:T(8,128)(2,1)} %all-gather.8.cloned.1.call-done), kind=kOutput, calls=%fused_computation.14 | convolution fusion | flops 2164260864 | bytes 8077312 | tf_op jit(solution)/shard_map/dot_general | solution.py:132
  240.3 11.7 %convolution_convert_fusion = bf16[768,2048]{1,0:T(8,128)(2,1)} fusion(bf16[2048,2064]{0,1:T(8,128)(2,1)} %all-gather.8.cloned.1.call-done, f32[768,688]{0,1:T(8,128)S(1)} %fusion.9, bf16[768,2048]{1,0:T(8,128)(2,1)} %bitcast.47), kind=kOutput, calls=%fused_computation.9 | convolution fusion | flops 4333264896 | bytes 14041088 | tf_op jit(solution)/shard_map/dot_general | solution.py:135
  252.0 0.0 reduce-scatter.3.cloned.1.call-update
  252.0 0.0 reduce-scatter.5.cloned.1.call-start
  252.0 36.7 %reduce-scatter.3.cloned.1.call-done = bf16[192,2048]{1,0:T(8,128)(2,1)} async-done(((bf16[768,2048]{1,0:T(8,128)(2,1)}), bf16[192,2048]{1,0:T(8,128)(2,1)}) %reduce-scatter.3.cloned.1.call-update) | async-done | bytes 786448 | tf_op jit(solution)/shard_map/reduce_scatter | solution.py:55
  288.7 0.0 reduce-scatter.5.cloned.1.call-update
  288.7 13.3 %reduce-scatter.5.cloned.1.call-done = bf16[96,2048]{1,0:T(8,128)(2,1)} async-done(((bf16[192,2048]{1,0:T(8,128)(2,1)}), bf16[96,2048]{1,0:T(8,128)(2,1)}) %reduce-scatter.5.cloned.1.call-update) | async-done | bytes 393232 | tf_op jit(solution)/shard_map/reduce_scatter | solution.py:55
  302.0 1.9 add_convert_fusion
  (3 shorter events, 0.0 us)
Async XLA Ops:
  6.5 67.4 %all-gather.4.cloned.1.call-start = ((), (), s32[]{:S(2)}) async-start(), calls=%async_computation.5 | async-start | bytes 6684672 | tf_op jit(solution)/shard_map/all_gather | solution.py:50
  8.3 20.0 %copy-start.2 = (bf16[768,128]{1,0:T(8,128)(2,1)S(1)}, bf16[768,128]{1,0:T(8,128)(2,1)}, u32[]{:S(2)}) copy-start(bf16[768,128]{1,0:T(8,128)(2,1)} %param.11) | copy-start | bytes 589828
  8.4 175.4 %all-gather.6.cloned.1.call-start = ((), (), s32[]{:S(2)}) async-start(), calls=%async_computation.6 | async-start | bytes 4718592 | tf_op jit(solution)/shard_map/all_gather | solution.py:86
  10.5 72.4 %all-to-all-start = ((f32[16,768,2]{1,2,0:T(2,128)}), f32[16,768,2]{1,2,0:T(2,128)S(1)}, u32[]{:S(2)}, u32[]{:S(2)}) async-start(f32[16,768,2]{1,2,0:T(2,128)} %broadcast_in_dim.17), calls=%async_computation | async-start | bytes 196608 | tf_op jit(solution)/shard_map/all_to_all | solution.py:35
  18.9 216.2 %all-gather.8.cloned.1.call-start = ((), (), s32[]{:S(2)}) async-start(), calls=%async_computation.7 | async-start | bytes 8982528 | tf_op jit(solution)/shard_map/all_gather | solution.py:17
  78.2 4.7 %copy-start.3 = (f32[768,2]{0,1:T(2,128)S(1)}, f32[768,2]{0,1:T(2,128)}, u32[]{:S(2)}) copy-start(f32[768,2]{0,1:T(2,128)} %param.14) | copy-start | bytes 18436
  119.0 27.8 %copy-start.1 = (bf16[12288,128]{0,1:T(8,128)(2,1)S(1)}, bf16[12288,128]{0,1:T(8,128)(2,1)}, u32[]{:S(2)}) copy-start(bf16[12288,128]{0,1:T(8,128)(2,1)} %copy.23) | copy-start | bytes 9437188
  177.5 15.3 %copy-start = (bf16[96,2048]{1,0:T(8,128)(2,1)S(1)}, bf16[96,2048]{1,0:T(8,128)(2,1)}, u32[]{:S(2)}) copy-start(bf16[96,2048]{1,0:T(8,128)(2,1)} %param.10) | copy-start | bytes 1179652
  177.5 15.5 %copy-start.4 = (f32[2048]{0:T(1024)S(1)}, f32[2048]{0:T(1024)}, u32[]{:S(2)}) copy-start(f32[2048]{0:T(1024)} %param.16) | copy-start | bytes 24580
  178.7 10.9 %all-to-all-start.1 = ((bf16[8,96,128]{2,1,0:T(8,128)(2,1)}), bf16[8,96,128]{2,1,0:T(8,128)(2,1)S(1)}, u32[]{:S(2)}, u32[]{:S(2)}) async-start(bf16[8,96,128]{2,1,0:T(8,128)(2,1)} %copy.25), calls=%async_computation.1 | async-start | bytes 393216 | tf_op jit(solution)/shard_map/all_to_all | solution.py:120
  183.7 105.0 %reduce-scatter.3.cloned.1.call-start = ((), (), s32[]{:S(2)}) async-start(), calls=%async_computation.8 | async-start | bytes 3932160 | tf_op jit(solution)/shard_map/reduce_scatter | solution.py:55
  252.0 50.0 %reduce-scatter.5.cloned.1.call-start = ((), (), s32[]{:S(2)}) async-start(), calls=%async_computation.9 | async-start | bytes 1179648 | tf_op jit(solution)/shard_map/reduce_scatter | solution.py:55
Sparse Core Ops, SparseCore 0:
  9.5 64.4 all-gather.3
  75.7 32.1 all-gather.5
  110.0 75.6 all-gather.7
  252.1 36.5 reduce-scatter.2
  290.9 11.0 reduce-scatter.4
